TPU v7x, 32 devices: a whole 2x2x4 slice. The times are simulated.
32 devices in a mesh: ep: 8 (over z, y), tp: 4 (over x, core).
Axes of the slice: x: 2, y: 2, z: 4, core: 2. Of those that a mesh axis runs over, the one named last changes fastest.
Arguments:
- tokens: bfloat16 [1024, 2048], P('ep', 'tp'), may hold values from -6 to 6
- norm_gain: bfloat16 [2048], P('tp'), may hold values from 0.099609375 to 1.8984375
- routes: int32 [1024, 2], P('ep'), may hold values from 0 to 7, as said below
- gate_weights: float32 [1024, 2], P('ep'), may hold values from 0.1 to 1
- w_gate: bfloat16 [8, 2048, 4096], P('ep', None, 'tp'), may hold values from -0.125 to 0.125
- w_up: bfloat16 [8, 2048, 4096], P('ep', None, 'tp'), may hold values from -0.125 to 0.125
- w_down: bfloat16 [8, 4096, 2048], P('ep', 'tp'), may hold values from -0.875 to 0.875
- out_gain: bfloat16 [2048], P('tp'), may hold values from 0.099609375 to 1.8984375
Outputs:
- mixed: bfloat16 [1024, 2048], P('ep', 'tp')
Inputs may be any that keep to these rules, and one draw needn't show every extreme that they name: `routes`: each row names 2 different experts of one group (their quotients by 8 agree). In each aligned block of 128 rows no expert is named by more than 64 rows, and in every block some expert is named by exactly 64 rows.
All inputs are finite; a program needn't handle non-finite values.
Results may differ from a plain program's by a relative error of at most 0.019.
Values may be sent and summed in bfloat16 or wider, within the bound.
A program may use at most 64 MiB of HBM per device.

v0:
```python
import functools

import jax
import jax.numpy as jnp
from jax import lax
from jax.experimental import pallas as pl
from jax.experimental.pallas import tpu as pltpu
from jax.sharding import PartitionSpec as P

epsilon = 1e-06
CORES = 2


def shards(tokens, norm_gain, routes, gate_weights, w_gate, w_up, w_down, out_gain):
    tok_rows = tokens.shape[0]
    width_local = tokens.shape[1]
    full_width = width_local * lax.axis_size("tp")
    experts = lax.axis_size("ep")
    top_count = routes.shape[1]
    capacity = 2 * top_count * tok_rows // experts
    flat_ids = routes.reshape(-1)
    onehot = (flat_ids[:, None] == jnp.arange(experts, dtype=jnp.int32)[None, :]).astype(jnp.int32)
    before = jnp.cumsum(onehot, axis=0) - onehot
    slot_index = jnp.sum(before * onehot, axis=1)
    dest_index = flat_ids * capacity + slot_index
    dest_pairs = dest_index.reshape(tok_rows, top_count)
    places = jnp.arange(experts * capacity, dtype=jnp.int32)
    scatter_mat = jnp.any(dest_pairs[None, :, :] == places[:, None, None], axis=2).astype(
        jnp.bfloat16
    )
    gate_mat = w_gate[0]
    up_mat = w_up[0]
    x_float = tokens.astype(jnp.float32)
    row_sums = lax.psum(jnp.sum(x_float * x_float, axis=1), "tp")
    scale_in = lax.rsqrt(row_sums / full_width + epsilon)
    normed = (x_float * scale_in[:, None] * norm_gain.astype(jnp.float32)).astype(jnp.bfloat16)
    outgoing = jnp.dot(scatter_mat, normed, preferred_element_type=jnp.float32).astype(jnp.bfloat16)
    arrived = lax.all_to_all(outgoing, "ep", split_axis=0, concat_axis=0, tiled=True)
    portion = lax.all_gather(arrived, "tp", axis=1, tiled=True)
    gate_sum = jnp.dot(portion, gate_mat, preferred_element_type=jnp.float32)
    up_sum = jnp.dot(portion, up_mat, preferred_element_type=jnp.float32)
    hidden = (jax.nn.silu(gate_sum) * up_sum).astype(jnp.bfloat16)
    down_mat = w_down[0]
    summed = lax.psum_scatter(
        lax.dot_general(
            down_mat, hidden, (((0,), (1,)), ((), ())), preferred_element_type=jnp.float32
        ).astype(jnp.bfloat16),
        "tp",
        scatter_dimension=0,
        tiled=True,
    )
    came_back = lax.all_to_all(summed, "ep", split_axis=1, concat_axis=1, tiled=True)
    picked = (
        jnp.take(came_back, dest_index, axis=1)
        .astype(jnp.float32)
        .reshape(width_local, tok_rows, top_count)
    )
    combined = jnp.sum(picked * gate_weights[None, :, :], axis=2).T
    out_sums = lax.psum(jnp.sum(combined * combined, axis=1), "tp")
    scale_out = lax.rsqrt(out_sums / full_width + epsilon)
    return (combined * scale_out[:, None] * out_gain.astype(jnp.float32)).astype(jnp.bfloat16)


def xor(index, mask):
    result = index
    bit = 1
    while bit <= mask:
        if mask & bit:
            result = result + bit * (1 - 2 * ((index // bit) % 2))
        bit *= 2
    return result


def layer(
    n_ep, cap, near,
    routes_ref, gates_ref, tokens_ref, in_gain_ref, out_gain_ref, wg_hbm, wu_hbm, wd_hbm,
    out_ref,
    wg, wu, wd, picked, xall, gains, xn, hidden, psend, prec, own, xsend, xrec, rsend, back, sums,
    w_sem, disp_s, disp_r, part_s, part_r, opp_s, opp_r, rel_s, rel_r, gain_s, gain_r,
    pd_s, pd_r, xs_s, xs_r, ret_s, ret_r, ns_s, ns_r,
):
    f32, bf16 = jnp.float32, jnp.bfloat16
    ep, tp = lax.axis_index("ep"), lax.axis_index("tp")
    chip, core = tp // CORES, tp % CORES
    partner = chip * CORES + (1 - core)
    opposite = (1 - chip) * CORES + core
    diagonal = (1 - chip) * CORES + (1 - core)
    tok, width = tokens_ref.shape
    n_tp = gains.shape[0]
    full = width * n_tp
    ff = wg.shape[1]
    half_rows = n_ep // 2 * cap
    source = [xor(ep, d) for d in range(n_ep)]
    rows = [pl.ds(pl.multiple_of(s * cap, cap), cap) for s in source]
    my_rows = rows[0]

    barrier = pltpu.get_barrier_semaphore()
    for d in range(1, n_ep):
        pl.semaphore_signal(barrier, inc=1, device_id={"ep": source[d]})
    for peer in (partner, opposite, diagonal):
        pl.semaphore_signal(barrier, inc=1, device_id={"tp": peer})

    weights = [
        pltpu.make_async_copy(src.at[0], dst, w_sem.at[i])
        for i, (src, dst) in enumerate(((wg_hbm, wg), (wu_hbm, wu), (wd_hbm, wd)))
    ]
    for copy in weights:
        copy.start()

    def remote(src, dst, send, recv, where):
        return pltpu.make_async_remote_copy(
            src_ref=src, dst_ref=dst, send_sem=send, recv_sem=recv, device_id=where
        )

    diag = lax.broadcasted_iota(jnp.int32, (tok, tok), 0) == lax.broadcasted_iota(
        jnp.int32, (tok, tok), 1
    )

    def column(row):
        return jnp.sum(jnp.where(diag, row, 0.0), axis=1, keepdims=True)

    routes = routes_ref[...].astype(f32)
    first, second = column(routes[0:1]), column(routes[1:2])
    lanes = 128 * pl.cdiv(n_ep, 128)
    expert = lax.broadcasted_iota(jnp.int32, (tok, lanes), 1).astype(f32)
    is_first, is_second = expert == first, expert == second
    member = jnp.where(is_first, 1.0, 0.0) + jnp.where(is_second, 1.0, 0.0)
    earlier = jnp.where(
        lax.broadcasted_iota(jnp.int32, (tok, tok), 1)
        < lax.broadcasted_iota(jnp.int32, (tok, tok), 0),
        1.0,
        0.0,
    )
    before = jnp.dot(earlier.astype(bf16), member.astype(bf16), preferred_element_type=f32)
    place = before + expert * cap
    place_first = jnp.sum(jnp.where(is_first, place, 0.0), axis=1, keepdims=True)
    place_second = jnp.sum(jnp.where(is_second, place, 0.0), axis=1, keepdims=True)
    slots = lax.broadcasted_iota(jnp.int32, (tok, n_ep * cap), 1).astype(f32)
    at_first, at_second = slots == place_first, slots == place_second
    select = (jnp.where(at_first, 1.0, 0.0) + jnp.where(at_second, 1.0, 0.0)).astype(bf16)
    picked[...] = lax.dot_general(
        select, tokens_ref[...], (((0,), (0,)), ((), ())), preferred_element_type=f32
    ).astype(bf16)
    gains[pl.ds(tp, 1)] = in_gain_ref[...].astype(f32).reshape(1, 1, width)
    xall[pl.ds(tp, 1), my_rows] = picked[my_rows][None]

    pl.semaphore_wait(barrier, n_ep - 1 + n_tp - 1)

    dispatch = {
        d: remote(picked.at[rows[d]], xall.at[tp, my_rows], disp_s.at[d], disp_r.at[d], {"ep": source[d]})
        for d in range(1, n_ep)
    }
    to_partner, to_opposite, relay = [], [], []
    for d in range(n_ep):
        block = xall.at[tp, rows[d]]
        to_partner.append(remote(block, block, part_s.at[d], part_r.at[d], {"tp": partner}))
        to_opposite.append(remote(block, block, opp_s.at[d], opp_r.at[d], {"tp": opposite}))
        far = xall.at[opposite, rows[d]]
        relay.append(remote(far, far, rel_s.at[d], rel_r.at[d], {"tp": partner}))
    gain_copies = [
        remote(gains.at[tp], gains.at[tp], gain_s.at[i], gain_r.at[i], {"tp": peer})
        for i, peer in enumerate((partner, opposite, diagonal))
    ]
    for copy in gain_copies:
        copy.start()
    to_opposite[0].start()
    to_partner[0].start()
    order = near[1:]
    for d in order:
        dispatch[d].start()

    def forward(d):
        dispatch[d].wait_recv()
        to_opposite[d].start()
        to_partner[d].start()

    def pass_on(d):
        to_opposite[d].wait_recv()
        relay[d].start()

    def normalise(i, d):
        to_partner[d].wait_recv()
        relay[d].wait_recv()
        parts = [xall[j, rows[d]].astype(f32) for j in range(n_tp)]
        total = sum(jnp.sum(p * p, axis=1, keepdims=True) for p in parts)
        scale = lax.rsqrt(total / full + epsilon)
        for j in range(n_tp):
            xn[i * cap : (i + 1) * cap, j * width : (j + 1) * width] = (
                parts[j] * scale * gains[j]
            ).astype(bf16)

    tile = min(256, ff)
    tiles = ff // tile

    def units(h, start, stop):
        mine = slice(h * half_rows, (h + 1) * half_rows)

        def body(n, carry):
            cols = pl.ds(pl.multiple_of(n * tile, tile), tile)
            gate = jnp.dot(xn[mine], wg[:, cols], preferred_element_type=f32)
            up = jnp.dot(xn[mine], wu[:, cols], preferred_element_type=f32)
            hidden[mine, cols] = (gate / (1.0 + jnp.exp(-gate)) * up).astype(bf16)
            return carry

        lax.fori_loop(start, stop, body, 0)

    far_partner, near_partner = diagonal, partner
    partner_copies = {
        (h, k): remote(psend.at[h, k], prec.at[h, k], pd_s.at[h, k], pd_r.at[h, k], {"tp": partner})
        for h in range(2)
        for k in range(2)
    }

    def down(h):
        mine = slice(h * half_rows, (h + 1) * half_rows)

        def product(j):
            cols = pl.ds(pl.multiple_of(j * width, width), width)
            return jnp.dot(hidden[mine], wd[:, cols], preferred_element_type=f32)

        for k, j in enumerate((far_partner, near_partner)):
            psend[h, k] = product(j).astype(bf16)
            partner_copies[h, k].start()
        for k, j in enumerate((opposite, tp)):
            own[h, k] = product(j)

    across = [
        remote(xsend.at[i], xrec.at[i], xs_s.at[i], xs_r.at[i], {"tp": opposite})
        for i in range(n_ep)
    ]
    returned = {
        d: remote(rsend.at[d], back.at[my_rows], ret_s.at[d], ret_r.at[d], {"ep": source[d]})
        for d in range(1, n_ep)
    }

    def send_across(h):
        partner_copies[h, 0].wait_recv()
        for q in range(n_ep // 2):
            i = h * (n_ep // 2) + q
            part = slice(q * cap, (q + 1) * cap)
            xsend[i] = (own[h, 0, part] + prec[h, 0, part].astype(f32)).astype(bf16)
            across[i].start()

    def send_back(i):
        h, q = divmod(i, n_ep // 2)
        d = near[i]
        part = slice(q * cap, (q + 1) * cap)
        both = own[h, 1, part] + prec[h, 1, part].astype(f32)
        across[i].wait_recv()
        done = (both + xrec[i].astype(f32)).astype(bf16)
        if d == 0:
            back[my_rows] = done
        else:
            rsend[d] = done
            returned[d].start()

    half = n_ep // 2
    group_a, group_b = near[:half], near[half:]
    for copy in gain_copies:
        copy.wait_recv()
    for i in range(1, half):
        forward(group_a[i])
    for d in group_a:
        pass_on(d)
    for i, d in enumerate(group_a):
        normalise(i, d)
    for copy in weights[:2]:
        copy.wait()
    pieces = min(half, tiles)
    done = 0
    for piece in range(pieces):
        until = (piece + 1) * half // pieces
        for i in range(done, until):
            forward(group_b[i])
            if i:
                pass_on(group_b[i - 1])
        done = until
        units(0, piece * tiles // pieces, (piece + 1) * tiles // pieces)
    pass_on(group_b[half - 1])
    weights[2].wait()
    down(0)
    send_across(0)
    for i, d in enumerate(group_b):
        normalise(half + i, d)
    partner_copies[0, 1].wait_recv()
    done = 0
    for piece in range(pieces):
        units(1, piece * tiles // pieces, (piece + 1) * tiles // pieces)
        until = (piece + 1) * half // pieces
        for i in range(done, until):
            send_back(i)
        done = until
    down(1)
    send_across(1)
    partner_copies[1, 1].wait_recv()
    for i in range(half, n_ep):
        send_back(i)

    gates = gates_ref[...]
    mixing = jnp.where(at_first, column(gates[0:1]), 0.0) + jnp.where(
        at_second, column(gates[1:2]), 0.0
    )
    high = mixing.astype(bf16)
    low = (mixing - high.astype(f32)).astype(bf16)
    for d in range(1, n_ep):
        returned[d].wait_recv()
    rows_back = back[...]
    combined = jnp.dot(high, rows_back, preferred_element_type=f32) + jnp.dot(
        low, rows_back, preferred_element_type=f32
    )
    row_sum = jnp.sum(combined * combined, axis=1, keepdims=True)
    flat = jnp.sum(jnp.where(diag, row_sum, 0.0), axis=0, keepdims=True)
    sums[pl.ds(tp, 1)] = flat[None]
    norm_copies = [
        remote(sums.at[tp], sums.at[tp], ns_s.at[i], ns_r.at[i], {"tp": peer})
        for i, peer in enumerate((partner, opposite, diagonal))
    ]
    for copy in norm_copies:
        copy.start()

    for copy in gain_copies + to_partner + to_opposite + relay + across:
        copy.wait_send()
    for copies in (dispatch, partner_copies, returned):
        for copy in copies.values():
            copy.wait_send()

    for copy in norm_copies:
        copy.wait()
    total = sum(sums[j] for j in range(n_tp))
    scale = lax.rsqrt(column(total) / full + epsilon)
    gain = out_gain_ref[...].astype(f32).reshape(1, width)
    out_ref[...] = (combined * scale * gain).astype(bf16)


def fused(tokens, norm_gain, routes, gate_weights, w_gate, w_up, w_down, out_gain):
    n_ep, n_tp = lax.axis_size("ep"), lax.axis_size("tp")
    tok, width = tokens.shape
    cap = 2 * routes.shape[1] * tok // n_ep
    _, d_model, ff = w_gate.shape
    half_rows = n_ep // 2 * cap
    near = tuple(range(0, n_ep, 2)) + tuple(range(1, n_ep, 2))
    bf16, f32 = jnp.bfloat16, jnp.float32
    dma = pltpu.SemaphoreType.DMA
    vmem = pl.BlockSpec(memory_space=pltpu.VMEM)
    anywhere = pl.BlockSpec(memory_space=pl.ANY)
    slots = n_ep * cap
    return pl.pallas_call(
        functools.partial(layer, n_ep, cap, near),
        out_shape=jax.ShapeDtypeStruct((tok, width), bf16),
        in_specs=[vmem] * 5 + [anywhere] * 3,
        out_specs=vmem,
        scratch_shapes=[
            pltpu.VMEM((d_model, ff), bf16),
            pltpu.VMEM((d_model, ff), bf16),
            pltpu.VMEM((ff, d_model), bf16),
            pltpu.VMEM((slots, width), bf16),
            pltpu.VMEM((n_tp, slots, width), bf16),
            pltpu.VMEM((n_tp, 1, width), f32),
            pltpu.VMEM((slots, d_model), bf16),
            pltpu.VMEM((slots, ff), bf16),
            pltpu.VMEM((2, 2, half_rows, width), bf16),
            pltpu.VMEM((2, 2, half_rows, width), bf16),
            pltpu.VMEM((2, 2, half_rows, width), f32),
            pltpu.VMEM((n_ep, cap, width), bf16),
            pltpu.VMEM((n_ep, cap, width), bf16),
            pltpu.VMEM((n_ep, cap, width), bf16),
            pltpu.VMEM((slots, width), bf16),
            pltpu.VMEM((n_tp, 1, tok), f32),
            dma((3,)),
            *[dma((n_ep,))] * 8,
            *[dma((3,))] * 2,
            *[dma((2, 2))] * 2,
            *[dma((n_ep,))] * 4,
            *[dma((3,))] * 2,
        ],
        compiler_params=pltpu.CompilerParams(
            collective_id=0, has_side_effects=True, vmem_limit_bytes=60 * 1024 * 1024
        ),
    )(
        routes.T, gate_weights.T, tokens, norm_gain, out_gain,
        w_gate, w_up, w_down,
    )


def solution(mesh):
    placed = (
        P("ep", "tp"),
        P("tp"),
        P("ep", None),
        P("ep", None),
        P("ep", None, "tp"),
        P("ep", None, "tp"),
        P("ep", "tp", None),
        P("tp"),
    )
    n_ep = mesh.shape["ep"]
    pairs = mesh.shape["tp"] == 2 * CORES and n_ep >= 8 and n_ep & (n_ep - 1) == 0
    return jax.shard_map(
        fused if pairs else shards, mesh=mesh, in_specs=placed, out_specs=P("ep", "tp"), check_vma=False
    )
```

profile of v0, /device:TPU:0, one launch (start us, length us, event | category | flops | bytes accessed | tf_op | source)
XLA Modules:
  0.0 59.7 jit_solution(17607183160198087295)
XLA Ops:
  0.0 58.1 %shard_map.82 = bf16[128,512]{1,0:T(8,128)(2,1)} custom-call(s32[2,128]{1,0:T(2,128)} %bitcast.2, f32[2,128]{1,0:T(2,128)} %bitcast.3, bf16[128,512]{1,0:T(8,128)(2,1)} %tokens_ref.1, bf16[512]{0:T(512)(128)(2,1)} %in_gain_ref.1, bf16[512]{0:T(512)(128)(2,1)} %out_gain_ref.1, bf16[1,2048,1024]{2,1,0:T(8,128)(2,1)} %wg_hbm.1, bf16[1,2048,1024]{2,1,0:T(8,128)(2,1)} %wu_hbm.1, ...), custom_call_target="tpu_custom_call" | custom-call | tf_op jit(solution)/shard_map/pallas_call | solution.py:347
  58.1 1.6 %copy.10 = bf16[128,512]{1,0:T(8,128)(2,1)} copy(bf16[128,512]{1,0:T(8,128)(2,1)} %shard_map.82) | data formatting | bytes 262144
where the time goes:
time: 59.8 us; the launch traced here: 59.7 us
  Pallas kernels  58.1 us (97%)
  local copies, waits for them, and re-layouts  1.57 us (3%)
    pallas_call x1, Pallas kernels, fused(): pl.pallas_call(functools.partial(layer, n_ep, cap, near), out_shape=jax.S...  58.1 us
    unnamed x1, local copies, waits for them, and re-layouts  1.57 us

commit v1 on v0

v1 whole, which is shorter than its diff:
```python
import functools

import jax
import jax.numpy as jnp
from jax import lax
from jax.experimental import pallas as pl
from jax.experimental.pallas import tpu as pltpu
from jax.sharding import PartitionSpec as P

epsilon = 1e-06
CORES = 2


def shards(tokens, norm_gain, routes, gate_weights, w_gate, w_up, w_down, out_gain):
    tok_rows = tokens.shape[0]
    width_local = tokens.shape[1]
    full_width = width_local * lax.axis_size("tp")
    experts = lax.axis_size("ep")
    top_count = routes.shape[1]
    capacity = 2 * top_count * tok_rows // experts
    flat_ids = routes.reshape(-1)
    onehot = (flat_ids[:, None] == jnp.arange(experts, dtype=jnp.int32)[None, :]).astype(jnp.int32)
    before = jnp.cumsum(onehot, axis=0) - onehot
    slot_index = jnp.sum(before * onehot, axis=1)
    dest_index = flat_ids * capacity + slot_index
    dest_pairs = dest_index.reshape(tok_rows, top_count)
    places = jnp.arange(experts * capacity, dtype=jnp.int32)
    scatter_mat = jnp.any(dest_pairs[None, :, :] == places[:, None, None], axis=2).astype(
        jnp.bfloat16
    )
    gate_mat = w_gate[0]
    up_mat = w_up[0]
    x_float = tokens.astype(jnp.float32)
    row_sums = lax.psum(jnp.sum(x_float * x_float, axis=1), "tp")
    scale_in = lax.rsqrt(row_sums / full_width + epsilon)
    normed = (x_float * scale_in[:, None] * norm_gain.astype(jnp.float32)).astype(jnp.bfloat16)
    outgoing = jnp.dot(scatter_mat, normed, preferred_element_type=jnp.float32).astype(jnp.bfloat16)
    arrived = lax.all_to_all(outgoing, "ep", split_axis=0, concat_axis=0, tiled=True)
    portion = lax.all_gather(arrived, "tp", axis=1, tiled=True)
    gate_sum = jnp.dot(portion, gate_mat, preferred_element_type=jnp.float32)
    up_sum = jnp.dot(portion, up_mat, preferred_element_type=jnp.float32)
    hidden = (jax.nn.silu(gate_sum) * up_sum).astype(jnp.bfloat16)
    down_mat = w_down[0]
    summed = lax.psum_scatter(
        lax.dot_general(
            down_mat, hidden, (((0,), (1,)), ((), ())), preferred_element_type=jnp.float32
        ).astype(jnp.bfloat16),
        "tp",
        scatter_dimension=0,
        tiled=True,
    )
    came_back = lax.all_to_all(summed, "ep", split_axis=1, concat_axis=1, tiled=True)
    picked = (
        jnp.take(came_back, dest_index, axis=1)
        .astype(jnp.float32)
        .reshape(width_local, tok_rows, top_count)
    )
    combined = jnp.sum(picked * gate_weights[None, :, :], axis=2).T
    out_sums = lax.psum(jnp.sum(combined * combined, axis=1), "tp")
    scale_out = lax.rsqrt(out_sums / full_width + epsilon)
    return (combined * scale_out[:, None] * out_gain.astype(jnp.float32)).astype(jnp.bfloat16)


def xor(index, mask):
    result = index
    bit = 1
    while bit <= mask:
        if mask & bit:
            result = result + bit * (1 - 2 * ((index // bit) % 2))
        bit *= 2
    return result


def plan(groups, tiles):
    steps = []

    def add(name, *args):
        steps.append((name, args))

    add("forward", 1)
    add("pass_on", 0)
    add("forward", 2)
    add("forward", 3)
    add("pass_on", 1)
    add("gain_wait")
    add("normalise", 0)
    add("pass_on", 2)
    add("normalise", 1)
    add("weight_wait", 0, 1)
    add("units", 0, 0, 2)
    add("forward", 4)
    add("pass_on", 3)
    add("units", 0, 2, 4)
    add("weight_wait", 2)
    for k in range(4):
        add("down", 0, k)
    add("normalise", 2)
    add("normalise", 3)
    add("forward", 5)
    add("across", 0)
    add("across", 1)
    add("units", 1, 0, 2)
    add("pass_on", 4)
    add("units", 1, 2, 4)
    for k in range(4):
        add("down", 1, k)
    add("pass_on", 5)
    add("forward", 6)
    add("back", 0)
    add("back", 1)
    add("normalise", 4)
    add("normalise", 5)
    add("across", 2)
    add("across", 3)
    add("units", 2, 0, 2)
    add("pass_on", 6)
    add("forward", 7)
    add("units", 2, 2, 4)
    for k in range(4):
        add("down", 2, k)
    add("across", 4)
    add("across", 5)
    add("back", 2)
    add("back", 3)
    add("normalise", 6)
    add("pass_on", 7)
    add("normalise", 7)
    add("units", 3, 0, 2)
    add("back", 4)
    add("units", 3, 2, 4)
    add("back", 5)
    for k in range(4):
        add("down", 3, k)
    add("across", 6)
    add("across", 7)
    add("gather", 0, 4)
    add("back", 6)
    add("back", 7)
    add("gather", 4, 8)
    return steps


def layer(
    n_ep, cap, groups,
    routes_hbm, gates_hbm, tokens_hbm, in_gain_hbm, out_gain_hbm, wg_hbm, wu_hbm, wd_hbm,
    out_ref,
    routes_ref, gates_ref, tokens_ref, in_gain_ref, out_gain_ref,
    wg, wu, wd, picked, xall, gains, xn, hidden, psend, prec, own, xsend, xrec, rsend, back, sums, acc,
    i_sem, w_sem, disp_s, disp_r, part_s, part_r, opp_s, opp_r, rel_s, rel_r, gain_s, gain_r,
    pd_s, pd_r, xs_s, xs_r, ret_s, ret_r, ns_s, ns_r,
):
    f32, bf16 = jnp.float32, jnp.bfloat16
    ep, tp = lax.axis_index("ep"), lax.axis_index("tp")
    chip, core = tp // CORES, tp % CORES
    partner = chip * CORES + (1 - core)
    opposite = (1 - chip) * CORES + core
    diagonal = (1 - chip) * CORES + (1 - core)
    tok, width = tokens_ref.shape
    n_tp = gains.shape[0]
    full = width * n_tp
    ff = wg.shape[1]
    peer = [xor(ep, d) for d in range(n_ep)]

    barrier = pltpu.get_barrier_semaphore()
    for d in range(1, n_ep):
        pl.semaphore_signal(barrier, inc=1, device_id={"ep": peer[d]})
    for other in (partner, opposite, diagonal):
        pl.semaphore_signal(barrier, inc=1, device_id={"tp": other})

    inputs = [
        pltpu.make_async_copy(src, dst, i_sem.at[i])
        for i, (src, dst) in enumerate(
            (
                (routes_hbm, routes_ref),
                (tokens_hbm, tokens_ref),
                (in_gain_hbm, in_gain_ref),
                (gates_hbm, gates_ref),
                (out_gain_hbm, out_gain_ref),
            )
        )
    ]
    weights = [
        pltpu.make_async_copy(src.at[0], dst, w_sem.at[i])
        for i, (src, dst) in enumerate(((wg_hbm, wg), (wu_hbm, wu), (wd_hbm, wd)))
    ]
    for copy in inputs + weights:
        copy.start()

    def remote(src, dst, send, recv, where):
        return pltpu.make_async_remote_copy(
            src_ref=src, dst_ref=dst, send_sem=send, recv_sem=recv, device_id=where
        )

    diag = lax.broadcasted_iota(jnp.int32, (tok, tok), 0) == lax.broadcasted_iota(
        jnp.int32, (tok, tok), 1
    )

    def column(row):
        return jnp.sum(jnp.where(diag, row, 0.0), axis=1, keepdims=True)

    inputs[0].wait()
    routes = routes_ref[...].astype(f32)
    first, second = column(routes[0:1]), column(routes[1:2])
    lanes = 128 * pl.cdiv(n_ep, 128)
    lane = lax.broadcasted_iota(jnp.int32, (tok, lanes), 1)
    expert = lane.astype(f32)
    is_first, is_second = expert == first, expert == second
    member = jnp.where(is_first, 1.0, 0.0) + jnp.where(is_second, 1.0, 0.0)
    earlier = jnp.where(
        lax.broadcasted_iota(jnp.int32, (tok, tok), 1)
        < lax.broadcasted_iota(jnp.int32, (tok, tok), 0),
        1.0,
        0.0,
    )
    before = jnp.dot(earlier.astype(bf16), member.astype(bf16), preferred_element_type=f32)
    place = before + (lane ^ ep).astype(f32) * cap
    place_first = jnp.sum(jnp.where(is_first, place, 0.0), axis=1, keepdims=True)
    place_second = jnp.sum(jnp.where(is_second, place, 0.0), axis=1, keepdims=True)
    slots = lax.broadcasted_iota(jnp.int32, (tok, n_ep * cap), 1).astype(f32)
    at_first, at_second = slots == place_first, slots == place_second
    select = (jnp.where(at_first, 1.0, 0.0) + jnp.where(at_second, 1.0, 0.0)).astype(bf16)
    inputs[1].wait()
    chosen = lax.dot_general(
        select, tokens_ref[...], (((0,), (0,)), ((), ())), preferred_element_type=f32
    ).astype(bf16)
    xall[pl.ds(tp, 1), 0] = chosen[:cap][None]
    picked[...] = chosen
    inputs[2].wait()
    gains[pl.ds(tp, 1)] = in_gain_ref[...].astype(f32).reshape(1, 1, width)

    pl.semaphore_wait(barrier, n_ep - 1 + n_tp - 1)

    dispatch = {
        d: remote(
            picked.at[pl.ds(d * cap, cap)], xall.at[tp, d], disp_s.at[d], disp_r.at[d], {"ep": peer[d]}
        )
        for d in range(1, n_ep)
    }
    to_partner, to_opposite, relay = [], [], []
    for d in range(n_ep):
        block = xall.at[tp, d]
        to_partner.append(remote(block, block, part_s.at[d], part_r.at[d], {"tp": partner}))
        to_opposite.append(remote(block, block, opp_s.at[d], opp_r.at[d], {"tp": opposite}))
        far = xall.at[opposite, d]
        relay.append(remote(far, far, rel_s.at[d], rel_r.at[d], {"tp": partner}))
    gain_copies = [
        remote(gains.at[tp], gains.at[tp], gain_s.at[i], gain_r.at[i], {"tp": other})
        for i, other in enumerate((partner, opposite, diagonal))
    ]
    for d in range(1, n_ep):
        dispatch[d].start()
    to_opposite[0].start()
    to_partner[0].start()
    for copy in gain_copies:
        copy.start()

    gates = gates_ref
    group_of, where_of = {}, {}
    begin = 0
    span = []
    for g, group in enumerate(groups):
        span.append(slice(begin * cap, (begin + len(group)) * cap))
        for q, d in enumerate(group):
            group_of[d], where_of[d] = (g, q), begin + q
        begin += len(group)
    tile = min(256, ff)
    partner_copies = {
        (g, k): remote(
            psend.at[k, span[g]], prec.at[k, span[g]], pd_s.at[g, k], pd_r.at[g, k], {"tp": partner}
        )
        for g in range(len(groups))
        for k in range(2)
    }
    across = [
        remote(xsend.at[d], xrec.at[d], xs_s.at[d], xs_r.at[d], {"tp": opposite})
        for d in range(n_ep)
    ]
    returned = {
        d: remote(rsend.at[d], back.at[pl.ds(d * cap, cap)], ret_s.at[d], ret_r.at[d], {"ep": peer[d]})
        for d in range(1, n_ep)
    }

    def forward(d):
        dispatch[d].wait_recv()
        to_opposite[d].start()
        to_partner[d].start()

    def pass_on(d):
        to_opposite[d].wait_recv()
        relay[d].start()

    def gain_wait():
        for copy in gain_copies:
            copy.wait_recv()

    def weight_wait(*which):
        for i in which:
            weights[i].wait()

    def normalise(d):
        to_partner[d].wait_recv()
        relay[d].wait_recv()
        parts = [xall[j, d].astype(f32) for j in range(n_tp)]
        total = sum(jnp.sum(p * p, axis=1, keepdims=True) for p in parts)
        scale = lax.rsqrt(total / full + epsilon)
        i = where_of[d]
        for j in range(n_tp):
            xn[i * cap : (i + 1) * cap, j * width : (j + 1) * width] = (
                parts[j] * scale * gains[j]
            ).astype(bf16)

    def units(g, start, stop):
        mine = span[g]

        def body(n, carry):
            cols = pl.ds(pl.multiple_of(n * tile, tile), tile)
            gate = jnp.dot(xn[mine], wg[:, cols], preferred_element_type=f32)
            up = jnp.dot(xn[mine], wu[:, cols], preferred_element_type=f32)
            hidden[mine, cols] = (gate / (1.0 + jnp.exp(-gate)) * up).astype(bf16)
            return carry

        lax.fori_loop(start, stop, body, 0)

    targets = (diagonal, partner, opposite, tp)

    def down(g, k):
        mine = span[g]
        cols = pl.ds(pl.multiple_of(targets[k] * width, width), width)
        product = jnp.dot(hidden[mine], wd[:, cols], preferred_element_type=f32)
        if k < 2:
            psend[k, mine] = product.astype(bf16)
            partner_copies[g, k].start()
        else:
            own[k - 2, mine] = product

    def rows_of(d):
        i = where_of[d]
        return slice(i * cap, (i + 1) * cap)

    def send_across(d):
        g, q = group_of[d]
        if q == 0:
            partner_copies[g, 0].wait_recv()
        part = rows_of(d)
        xsend[d] = (own[0, part] + prec[0, part].astype(f32)).astype(bf16)
        across[d].start()

    def send_back(d):
        g, q = group_of[d]
        if q == 0:
            partner_copies[g, 1].wait_recv()
        part = rows_of(d)
        both = own[1, part] + prec[1, part].astype(f32)
        across[d].wait_recv()
        done = (both + xrec[d].astype(f32)).astype(bf16)
        if d == 0:
            back[0:cap] = done
        else:
            rsend[d] = done
            returned[d].start()

    def mixing(d0, d1):
        cols = slice(d0 * cap, d1 * cap)
        part = jnp.where(at_first[:, cols], column(gates[0:1]), 0.0) + jnp.where(
            at_second[:, cols], column(gates[1:2]), 0.0
        )
        high = part.astype(bf16)
        low = (part - high.astype(f32)).astype(bf16)
        return high, low

    def gather(d0, d1):
        if d0 == 0:
            inputs[3].wait()
        for d in range(max(d0, 1), d1):
            returned[d].wait_recv()
        high, low = mixing(d0, d1)
        rows = back[d0 * cap : d1 * cap]
        total = jnp.dot(high, rows, preferred_element_type=f32) + jnp.dot(
            low, rows, preferred_element_type=f32
        )
        if d0:
            total = total + acc[...]
        if d1 < n_ep:
            acc[...] = total
        else:
            return total

    calls = dict(
        forward=forward, pass_on=pass_on, gain_wait=gain_wait, weight_wait=weight_wait, normalise=normalise,
        units=units, down=down, across=send_across, back=send_back, gather=gather,
    )
    combined = None
    for name, args in plan(groups, ff // tile):
        combined = calls[name](*args)

    row_sum = jnp.sum(combined * combined, axis=1, keepdims=True)
    flat = jnp.sum(jnp.where(diag, row_sum, 0.0), axis=0, keepdims=True)
    sums[pl.ds(tp, 1)] = flat[None]
    norm_copies = [
        remote(sums.at[tp], sums.at[tp], ns_s.at[i], ns_r.at[i], {"tp": other})
        for i, other in enumerate((partner, opposite, diagonal))
    ]
    for copy in norm_copies:
        copy.start()

    inputs[4].wait()
    for copy in gain_copies + to_partner + to_opposite + relay + across:
        copy.wait_send()
    for copies in (dispatch, partner_copies, returned):
        for copy in copies.values():
            copy.wait_send()

    for copy in norm_copies:
        copy.wait()
    total = sum(sums[j] for j in range(n_tp))
    scale = lax.rsqrt(column(total) / full + epsilon)
    gain = out_gain_ref[...].astype(f32).reshape(1, width)
    out_ref[...] = (combined * scale * gain).astype(bf16)


def fused(tokens, norm_gain, routes, gate_weights, w_gate, w_up, w_down, out_gain):
    n_ep, n_tp = lax.axis_size("ep"), lax.axis_size("tp")
    tok, width = tokens.shape
    top_count = routes.shape[1]
    cap = 2 * top_count * tok // n_ep
    _, d_model, ff = w_gate.shape
    groups = [(d, d + 1) for d in range(0, n_ep, 2)]
    bf16, f32 = jnp.bfloat16, jnp.float32
    dma = pltpu.SemaphoreType.DMA
    vmem = pl.BlockSpec(memory_space=pltpu.VMEM)
    hbm = pl.BlockSpec(memory_space=pltpu.HBM)
    slots = n_ep * cap
    return pl.pallas_call(
        functools.partial(layer, n_ep, cap, groups),
        out_shape=jax.ShapeDtypeStruct((tok, width), bf16),
        in_specs=[hbm] * 8,
        out_specs=vmem,
        scratch_shapes=[
            pltpu.VMEM((top_count, tok), jnp.int32),
            pltpu.VMEM((top_count, tok), f32),
            pltpu.VMEM((tok, width), bf16),
            pltpu.VMEM((width,), bf16),
            pltpu.VMEM((width,), bf16),
            pltpu.VMEM((d_model, ff), bf16),
            pltpu.VMEM((d_model, ff), bf16),
            pltpu.VMEM((ff, d_model), bf16),
            pltpu.VMEM((slots, width), bf16),
            pltpu.VMEM((n_tp, n_ep, cap, width), bf16),
            pltpu.VMEM((n_tp, 1, width), f32),
            pltpu.VMEM((slots, d_model), bf16),
            pltpu.VMEM((slots, ff), bf16),
            pltpu.VMEM((2, slots, width), bf16),
            pltpu.VMEM((2, slots, width), bf16),
            pltpu.VMEM((2, slots, width), f32),
            pltpu.VMEM((n_ep, cap, width), bf16),
            pltpu.VMEM((n_ep, cap, width), bf16),
            pltpu.VMEM((n_ep, cap, width), bf16),
            pltpu.VMEM((slots, width), bf16),
            pltpu.VMEM((n_tp, 1, tok), f32),
            pltpu.VMEM((tok, width), f32),
            dma((5,)),
            dma((3,)),
            *[dma((n_ep,))] * 8,
            *[dma((3,))] * 2,
            *[dma((len(groups), 2))] * 2,
            *[dma((n_ep,))] * 4,
            *[dma((3,))] * 2,
        ],
        compiler_params=pltpu.CompilerParams(
            collective_id=0, has_side_effects=True, vmem_limit_bytes=48 * 1024 * 1024
        ),
    )(
        *[
            pltpu.with_memory_space_constraint(x, pltpu.HBM)
            for x in (routes.T, gate_weights.T, tokens, norm_gain, out_gain, w_gate, w_up, w_down)
        ]
    )


def solution(mesh):
    placed = (
        P("ep", "tp"),
        P("tp"),
        P("ep", None),
        P("ep", None),
        P("ep", None, "tp"),
        P("ep", None, "tp"),
        P("ep", "tp", None),
        P("tp"),
    )
    n_ep = mesh.shape["ep"]
    pairs = mesh.shape["tp"] == 2 * CORES and n_ep >= 8 and n_ep & (n_ep - 1) == 0
    return jax.shard_map(
        fused if pairs else shards, mesh=mesh, in_specs=placed, out_specs=P("ep", "tp"), check_vma=False
    )
```

time: 59.8 us -> 49.8 us (0.83)
  Pallas kernels: 58.1 us -> 49 us
  local copies, waits for them, and re-layouts: 1.57 us -> 0.66 us
    pallas_call x1, Pallas kernels: 58.1 us -> 49 us  [fused(): pl.pallas_call(functools.partial(layer, n_ep, cap, groups), out_shape=jax...]
    unnamed x1, local copies, waits for them, and re-layouts: 1.57 us -> 0.66 us
where the time goes in v1:
time: 49.8 us; the launch traced here: 49.7 us
  Pallas kernels  49 us (98%)
  local copies, waits for them, and re-layouts  0.66 us (1%)
    pallas_call x1, Pallas kernels, fused(): pl.pallas_call(functools.partial(layer, n_ep, cap, groups), out_shape=jax...  49 us

profile of v1, /device:TPU:0, one launch (start us, length us, event | category | flops | bytes accessed | tf_op | source)
XLA Modules:
  0.0 49.7 jit_solution(14865798951653362484)
XLA Ops:
  0.0 49.0 %shard_map.82 = bf16[128,512]{1,0:T(8,128)(2,1)S(1)} custom-call(s32[2,128]{1,0:T(2,128)} %bitcast.2, f32[2,128]{1,0:T(2,128)} %bitcast.3, bf16[128,512]{1,0:T(8,128)(2,1)} %tokens_hbm.1, bf16[512]{0:T(512)(128)(2,1)} %in_gain_hbm.1, bf16[512]{0:T(512)(128)(2,1)} %out_gain_hbm.1, bf16[1,2048,1024]{2,1,0:T(8,128)(2,1)} %wg_hbm.1, ...), custom_call_target="tpu_custom_call" | custom-call | tf_op jit(solution)/shard_map/pallas_call | solution.py:433
  49.0 0.7 %copy.10 = bf16[128,512]{1,0:T(8,128)(2,1)} copy(bf16[128,512]{1,0:T(8,128)(2,1)S(1)} %shard_map.82) | data formatting | bytes 262144

commit v2 on v1

--- a/solution.py
+++ b/solution.py
@@ -71,7 +71,7 @@
     return result
 
 
-def plan(groups, tiles):
+def plan():
     steps = []
 
     def add(name, *args):
@@ -80,63 +80,71 @@
     add("forward", 1)
     add("pass_on", 0)
     add("forward", 2)
-    add("forward", 3)
     add("pass_on", 1)
     add("gain_wait")
     add("normalise", 0)
-    add("pass_on", 2)
+    add("forward", 3)
     add("normalise", 1)
     add("weight_wait", 0, 1)
-    add("units", 0, 0, 2)
+    add("gate", 0)
+    add("up", 0)
+    add("pass_on", 2)
     add("forward", 4)
+    add("weight_wait", 2)
+    add("down", 0, 0)
+    add("down", 0, 2)
+    add("down", 0, 1)
     add("pass_on", 3)
-    add("units", 0, 2, 4)
-    add("weight_wait", 2)
-    for k in range(4):
-        add("down", 0, k)
+    add("across", 0)
+    add("down", 0, 3)
     add("normalise", 2)
     add("normalise", 3)
     add("forward", 5)
-    add("across", 0)
+    add("pass_on", 4)
+    add("normalise", 4)
+    add("gate", 1)
+    add("forward", 6)
+    add("up", 1)
+    add("forward", 7)
+    add("down", 1, 0)
+    add("down", 1, 2)
+    add("down", 1, 1)
+    add("across", 4)
+    add("pass_on", 5)
+    add("down", 1, 3)
     add("across", 1)
-    add("units", 1, 0, 2)
-    add("pass_on", 4)
-    add("units", 1, 2, 4)
-    for k in range(4):
-        add("down", 1, k)
-    add("pass_on", 5)
-    add("forward", 6)
+    add("normalise", 5)
+    add("gate", 2)
+    add("pass_on", 6)
+    add("up", 2)
+    add("pass_on", 7)
+    add("down", 2, 0)
+    add("down", 2, 2)
+    add("normalise", 6)
+    add("down", 2, 1)
+    add("across", 5)
+    add("back", 4)
+    add("normalise", 7)
+    add("down", 2, 3)
+    add("across", 2)
+    add("gate", 3)
     add("back", 0)
-    add("back", 1)
-    add("normalise", 4)
-    add("normalise", 5)
-    add("across", 2)
-    add("across", 3)
-    add("units", 2, 0, 2)
-    add("pass_on", 6)
-    add("forward", 7)
-    add("units", 2, 2, 4)
-    for k in range(4):
-        add("down", 2, k)
-    add("across", 4)
-    add("across", 5)
-    add("back", 2)
-    add("back", 3)
-    add("normalise", 6)
-    add("pass_on", 7)
-    add("normalise", 7)
-    add("units", 3, 0, 2)
-    add("back", 4)
-    add("units", 3, 2, 4)
+    add("up", 3)
+    add("down", 3, 0)
+    add("down", 3, 2)
     add("back", 5)
-    for k in range(4):
-        add("down", 3, k)
+    add("down", 3, 1)
     add("across", 6)
     add("across", 7)
-    add("gather", 0, 4)
+    add("down", 3, 3)
+    add("across", 3)
+    add("back", 1)
+    add("back", 2)
     add("back", 6)
     add("back", 7)
-    add("gather", 4, 8)
+    add("back", 3)
+    add("gather", 0, 6)
+    add("gather", 6, 8)
     return steps
 
 
@@ -145,9 +153,8 @@
     routes_hbm, gates_hbm, tokens_hbm, in_gain_hbm, out_gain_hbm, wg_hbm, wu_hbm, wd_hbm,
     out_ref,
     routes_ref, gates_ref, tokens_ref, in_gain_ref, out_gain_ref,
-    wg, wu, wd, picked, xall, gains, xn, hidden, psend, prec, own, xsend, xrec, rsend, back, sums, acc,
-    i_sem, w_sem, disp_s, disp_r, part_s, part_r, opp_s, opp_r, rel_s, rel_r, gain_s, gain_r,
-    pd_s, pd_r, xs_s, xs_r, ret_s, ret_r, ns_s, ns_r,
+    wg, wu, wd, picked, xall, gains, xn, hidden, psend, prec, own, xsend, xrec, rsend, back, sums, acc, gated,
+    i_sem, w_sem, sent, disp_r, part_r, opp_r, gain_r, pd_r, xs_r, ret_r, ns_r,
 ):
     f32, bf16 = jnp.float32, jnp.bfloat16
     ep, tp = lax.axis_index("ep"), lax.axis_index("tp")
@@ -186,6 +193,9 @@
     for copy in inputs + weights:
         copy.start()
 
+    def wait_bytes(ref, sem):
+        pltpu.make_async_copy(ref, ref, sem).wait()
+
     def remote(src, dst, send, recv, where):
         return pltpu.make_async_remote_copy(
             src_ref=src, dst_ref=dst, send_sem=send, recv_sem=recv, device_id=where
@@ -232,51 +242,51 @@
 
     dispatch = {
         d: remote(
-            picked.at[pl.ds(d * cap, cap)], xall.at[tp, d], disp_s.at[d], disp_r.at[d], {"ep": peer[d]}
+            picked.at[pl.ds(d * cap, cap)], xall.at[tp, d], sent.at[0], disp_r.at[d], {"ep": peer[d]}
         )
         for d in range(1, n_ep)
     }
     to_partner, to_opposite, relay = [], [], []
     for d in range(n_ep):
         block = xall.at[tp, d]
-        to_partner.append(remote(block, block, part_s.at[d], part_r.at[d], {"tp": partner}))
-        to_opposite.append(remote(block, block, opp_s.at[d], opp_r.at[d], {"tp": opposite}))
+        to_partner.append(remote(block, block, sent.at[1], part_r.at[d], {"tp": partner}))
+        to_opposite.append(remote(block, block, sent.at[2], opp_r.at[d], {"tp": opposite}))
         far = xall.at[opposite, d]
-        relay.append(remote(far, far, rel_s.at[d], rel_r.at[d], {"tp": partner}))
+        relay.append(remote(far, far, sent.at[3], part_r.at[d], {"tp": partner}))
     gain_copies = [
-        remote(gains.at[tp], gains.at[tp], gain_s.at[i], gain_r.at[i], {"tp": other})
+        remote(gains.at[tp], gains.at[tp], sent.at[4], gain_r.at[0], {"tp": other})
         for i, other in enumerate((partner, opposite, diagonal))
     ]
-    for d in range(1, n_ep):
-        dispatch[d].start()
     to_opposite[0].start()
     to_partner[0].start()
+    for d in (1,2,3,4,5,6,7):
+        dispatch[d].start()
     for copy in gain_copies:
         copy.start()
 
     gates = gates_ref
+    part_of = {d: 0 if d < 6 else 1 for d in range(n_ep)}
     group_of, where_of = {}, {}
     begin = 0
     span = []
     for g, group in enumerate(groups):
         span.append(slice(begin * cap, (begin + len(group)) * cap))
         for q, d in enumerate(group):
-            group_of[d], where_of[d] = (g, q), begin + q
+            group_of[d], where_of[d] = g, begin + q
         begin += len(group)
-    tile = min(256, ff)
     partner_copies = {
         (g, k): remote(
-            psend.at[k, span[g]], prec.at[k, span[g]], pd_s.at[g, k], pd_r.at[g, k], {"tp": partner}
+            psend.at[k, span[g]], prec.at[k, span[g]], sent.at[5], pd_r.at[g, k], {"tp": partner}
         )
         for g in range(len(groups))
         for k in range(2)
     }
     across = [
-        remote(xsend.at[d], xrec.at[d], xs_s.at[d], xs_r.at[d], {"tp": opposite})
+        remote(xsend.at[d], xrec.at[d], sent.at[6], xs_r.at[d], {"tp": opposite})
         for d in range(n_ep)
     ]
     returned = {
-        d: remote(rsend.at[d], back.at[pl.ds(d * cap, cap)], ret_s.at[d], ret_r.at[d], {"ep": peer[d]})
+        d: remote(rsend.at[d], back.at[pl.ds(d * cap, cap)], sent.at[7], ret_r.at[part_of[d]], {"ep": peer[d]})
         for d in range(1, n_ep)
     }
 
@@ -290,16 +300,14 @@
         relay[d].start()
 
     def gain_wait():
-        for copy in gain_copies:
-            copy.wait_recv()
+        wait_bytes(gains.at[pl.ds(0, n_tp - 1)], gain_r.at[0])
 
     def weight_wait(*which):
         for i in which:
             weights[i].wait()
 
     def normalise(d):
-        to_partner[d].wait_recv()
-        relay[d].wait_recv()
+        wait_bytes(xall.at[pl.ds(0, CORES), d], part_r.at[d])
         parts = [xall[j, d].astype(f32) for j in range(n_tp)]
         total = sum(jnp.sum(p * p, axis=1, keepdims=True) for p in parts)
         scale = lax.rsqrt(total / full + epsilon)
@@ -309,17 +317,13 @@
                 parts[j] * scale * gains[j]
             ).astype(bf16)
 
-    def units(g, start, stop):
-        mine = span[g]
-
-        def body(n, carry):
-            cols = pl.ds(pl.multiple_of(n * tile, tile), tile)
-            gate = jnp.dot(xn[mine], wg[:, cols], preferred_element_type=f32)
-            up = jnp.dot(xn[mine], wu[:, cols], preferred_element_type=f32)
-            hidden[mine, cols] = (gate / (1.0 + jnp.exp(-gate)) * up).astype(bf16)
-            return carry
-
-        lax.fori_loop(start, stop, body, 0)
+    def gate(g):
+        gated[: cap * len(groups[g])] = jnp.dot(xn[span[g]], wg[...], preferred_element_type=f32)
+
+    def up(g):
+        value = gated[: cap * len(groups[g])]
+        product = jnp.dot(xn[span[g]], wu[...], preferred_element_type=f32)
+        hidden[span[g]] = (value / (1.0 + jnp.exp(-value)) * product).astype(bf16)
 
     targets = (diagonal, partner, opposite, tp)
 
@@ -333,22 +337,25 @@
         else:
             own[k - 2, mine] = product
 
+    waited = set()
+
+    def have(g, k):
+        if (g, k) not in waited:
+            waited.add((g, k))
+            partner_copies[g, k].wait_recv()
+
     def rows_of(d):
         i = where_of[d]
         return slice(i * cap, (i + 1) * cap)
 
     def send_across(d):
-        g, q = group_of[d]
-        if q == 0:
-            partner_copies[g, 0].wait_recv()
+        have(group_of[d], 0)
         part = rows_of(d)
         xsend[d] = (own[0, part] + prec[0, part].astype(f32)).astype(bf16)
         across[d].start()
 
     def send_back(d):
-        g, q = group_of[d]
-        if q == 0:
-            partner_copies[g, 1].wait_recv()
+        have(group_of[d], 1)
         part = rows_of(d)
         both = own[1, part] + prec[1, part].astype(f32)
         across[d].wait_recv()
@@ -371,8 +378,8 @@
     def gather(d0, d1):
         if d0 == 0:
             inputs[3].wait()
-        for d in range(max(d0, 1), d1):
-            returned[d].wait_recv()
+        lo = max(d0, 1)
+        wait_bytes(back.at[pl.ds(lo * cap, (d1 - lo) * cap)], ret_r.at[part_of[lo]])
         high, low = mixing(d0, d1)
         rows = back[d0 * cap : d1 * cap]
         total = jnp.dot(high, rows, preferred_element_type=f32) + jnp.dot(
@@ -387,31 +394,34 @@
 
     calls = dict(
         forward=forward, pass_on=pass_on, gain_wait=gain_wait, weight_wait=weight_wait, normalise=normalise,
-        units=units, down=down, across=send_across, back=send_back, gather=gather,
+        gate=gate, up=up, down=down, across=send_across, back=send_back, gather=gather,
     )
     combined = None
-    for name, args in plan(groups, ff // tile):
+    for name, args in plan():
         combined = calls[name](*args)
 
     row_sum = jnp.sum(combined * combined, axis=1, keepdims=True)
     flat = jnp.sum(jnp.where(diag, row_sum, 0.0), axis=0, keepdims=True)
     sums[pl.ds(tp, 1)] = flat[None]
     norm_copies = [
-        remote(sums.at[tp], sums.at[tp], ns_s.at[i], ns_r.at[i], {"tp": other})
+        remote(sums.at[tp], sums.at[tp], sent.at[8], ns_r.at[0], {"tp": other})
         for i, other in enumerate((partner, opposite, diagonal))
     ]
     for copy in norm_copies:
         copy.start()
 
     inputs[4].wait()
-    for copy in gain_copies + to_partner + to_opposite + relay + across:
-        copy.wait_send()
-    for copies in (dispatch, partner_copies, returned):
-        for copy in copies.values():
-            copy.wait_send()
-
-    for copy in norm_copies:
-        copy.wait()
+    blocks = xall.at[0]
+    wait_bytes(picked.at[pl.ds(0, (n_ep - 1) * cap)], sent.at[0])
+    for i in (1, 2, 3):
+        wait_bytes(blocks, sent.at[i])
+    wait_bytes(gains.at[pl.ds(0, n_tp - 1)], sent.at[4])
+    wait_bytes(psend, sent.at[5])
+    wait_bytes(xsend, sent.at[6])
+    wait_bytes(rsend.at[pl.ds(0, n_ep - 1)], sent.at[7])
+
+    wait_bytes(sums.at[pl.ds(0, n_tp - 1)], ns_r.at[0])
+    wait_bytes(sums.at[pl.ds(0, n_tp - 1)], sent.at[8])
     total = sum(sums[j] for j in range(n_tp))
     scale = lax.rsqrt(column(total) / full + epsilon)
     gain = out_gain_ref[...].astype(f32).reshape(1, width)
@@ -424,7 +434,7 @@
     top_count = routes.shape[1]
     cap = 2 * top_count * tok // n_ep
     _, d_model, ff = w_gate.shape
-    groups = [(d, d + 1) for d in range(0, n_ep, 2)]
+    groups = [(0,1),(2,4),(3,5),(6,7)]
     bf16, f32 = jnp.bfloat16, jnp.float32
     dma = pltpu.SemaphoreType.DMA
     vmem = pl.BlockSpec(memory_space=pltpu.VMEM)
@@ -458,13 +468,16 @@
             pltpu.VMEM((slots, width), bf16),
             pltpu.VMEM((n_tp, 1, tok), f32),
             pltpu.VMEM((tok, width), f32),
+            pltpu.VMEM((max(map(len, groups)) * cap, ff), f32),
             dma((5,)),
             dma((3,)),
-            *[dma((n_ep,))] * 8,
-            *[dma((3,))] * 2,
-            *[dma((len(groups), 2))] * 2,
-            *[dma((n_ep,))] * 4,
-            *[dma((3,))] * 2,
+            dma((9,)),
+            *[dma((n_ep,))] * 3,
+            dma((1,)),
+            dma((len(groups), 2)),
+            dma((n_ep,)),
+            dma((2,)),
+            dma((1,)),
         ],
         compiler_params=pltpu.CompilerParams(
             collective_id=0, has_side_effects=True, vmem_limit_bytes=48 * 1024 * 1024

time: 49.8 us -> 45.3 us (0.910)
  Pallas kernels: 49 us -> 44.5 us
    pallas_call x1, Pallas kernels: 49 us -> 44.5 us  [fused(): pl.pallas_call(functools.partial(layer, n_ep, cap, groups), out_shape=jax...]
where the time goes in v2:
time: 45.3 us; the launch traced here: 45.1 us
  Pallas kernels  44.5 us (98%)
  local copies, waits for them, and re-layouts  0.66 us (1%)
    pallas_call x1, Pallas kernels, fused(): pl.pallas_call(functools.partial(layer, n_ep, cap, groups), out_shape=jax...  44.5 us

profile of v2, /device:TPU:0, one launch (start us, length us, event | category | flops | bytes accessed | tf_op | source)
XLA Modules:
  0.0 45.1 jit_solution(9111250011201424190)
XLA Ops:
  0.0 44.5 %shard_map.82 = bf16[128,512]{1,0:T(8,128)(2,1)S(1)} custom-call(s32[2,128]{1,0:T(2,128)} %bitcast.2, f32[2,128]{1,0:T(2,128)} %bitcast.3, bf16[128,512]{1,0:T(8,128)(2,1)} %tokens_hbm.1, bf16[512]{0:T(512)(128)(2,1)} %in_gain_hbm.1, bf16[512]{0:T(512)(128)(2,1)} %out_gain_hbm.1, bf16[1,2048,1024]{2,1,0:T(8,128)(2,1)} %wg_hbm.1, ...), custom_call_target="tpu_custom_call" | custom-call | tf_op jit(solution)/shard_map/pallas_call | solution.py:443
  44.5 0.7 %copy.10 = bf16[128,512]{1,0:T(8,128)(2,1)} copy(bf16[128,512]{1,0:T(8,128)(2,1)S(1)} %shard_map.82) | data formatting | bytes 262144

commit v3 on v2

--- a/solution.py
+++ b/solution.py
@@ -9,6 +9,7 @@
 
 epsilon = 1e-06
 CORES = 2
+GROUPS = ((0, 1), (2, 4), (3, 5), (6, 7))
 
 
 def shards(tokens, norm_gain, routes, gate_weights, w_gate, w_up, w_down, out_gain):
@@ -78,44 +79,44 @@
         steps.append((name, args))
 
     add("forward", 1)
+    add("gain_wait")
+    add("pass_on", 1)
     add("pass_on", 0)
     add("forward", 2)
-    add("pass_on", 1)
-    add("gain_wait")
+    add("normalise", 1)
+    add("forward", 4)
+    add("weight_wait", 0, 1)
     add("normalise", 0)
+    add("gate", 0)
+    add("weight_wait", 2)
+    add("pass_on", 2)
     add("forward", 3)
-    add("normalise", 1)
-    add("weight_wait", 0, 1)
-    add("gate", 0)
     add("up", 0)
-    add("pass_on", 2)
-    add("forward", 4)
-    add("weight_wait", 2)
+    add("forward", 6)
+    add("pass_on", 4)
+    add("normalise", 2)
     add("down", 0, 0)
-    add("down", 0, 2)
-    add("down", 0, 1)
-    add("pass_on", 3)
-    add("across", 0)
-    add("down", 0, 3)
-    add("normalise", 2)
-    add("normalise", 3)
     add("forward", 5)
-    add("pass_on", 4)
     add("normalise", 4)
     add("gate", 1)
-    add("forward", 6)
     add("up", 1)
+    add("pass_on", 3)
     add("forward", 7)
     add("down", 1, 0)
+    add("down", 0, 1)
     add("down", 1, 2)
     add("down", 1, 1)
+    add("down", 0, 2)
     add("across", 4)
     add("pass_on", 5)
+    add("across", 1)
+    add("normalise", 3)
     add("down", 1, 3)
-    add("across", 1)
+    add("down", 0, 3)
     add("normalise", 5)
     add("gate", 2)
     add("pass_on", 6)
+    add("across", 0)
     add("up", 2)
     add("pass_on", 7)
     add("down", 2, 0)
@@ -125,24 +126,24 @@
     add("across", 5)
     add("back", 4)
     add("normalise", 7)
-    add("down", 2, 3)
+    add("gate", 3)
     add("across", 2)
-    add("gate", 3)
-    add("back", 0)
     add("up", 3)
     add("down", 3, 0)
     add("down", 3, 2)
-    add("back", 5)
+    add("down", 2, 3)
+    add("back", 1)
+    add("across", 7)
     add("down", 3, 1)
     add("across", 6)
-    add("across", 7)
+    add("across", 3)
+    add("back", 5)
+    add("back", 2)
     add("down", 3, 3)
-    add("across", 3)
-    add("back", 1)
-    add("back", 2)
+    add("back", 7)
     add("back", 6)
-    add("back", 7)
     add("back", 3)
+    add("back", 0)
     add("gather", 0, 6)
     add("gather", 6, 8)
     return steps
@@ -208,31 +209,35 @@
     def column(row):
         return jnp.sum(jnp.where(diag, row, 0.0), axis=1, keepdims=True)
 
+    def places(shape, tokens_at, first, second, count):
+        one = lax.broadcasted_iota(jnp.int32, shape, 1 - tokens_at)
+        expert = one.astype(f32)
+        is_first, is_second = expert == first, expert == second
+        member = jnp.where(is_first, 1.0, 0.0) + jnp.where(is_second, 1.0, 0.0)
+        place = count(member.astype(bf16)) + (one ^ ep).astype(f32) * cap
+        return tuple(
+            jnp.sum(jnp.where(chosen_one, place, 0.0), axis=1 - tokens_at, keepdims=True)
+            for chosen_one in (is_first, is_second)
+        )
+
+    later = jnp.where(
+        lax.broadcasted_iota(jnp.int32, (tok, tok), 0)
+        < lax.broadcasted_iota(jnp.int32, (tok, tok), 1),
+        1.0,
+        0.0,
+    ).astype(bf16)
+    slots = lax.broadcasted_iota(jnp.int32, (n_ep * cap, tok), 0).astype(f32)
     inputs[0].wait()
     routes = routes_ref[...].astype(f32)
-    first, second = column(routes[0:1]), column(routes[1:2])
-    lanes = 128 * pl.cdiv(n_ep, 128)
-    lane = lax.broadcasted_iota(jnp.int32, (tok, lanes), 1)
-    expert = lane.astype(f32)
-    is_first, is_second = expert == first, expert == second
-    member = jnp.where(is_first, 1.0, 0.0) + jnp.where(is_second, 1.0, 0.0)
-    earlier = jnp.where(
-        lax.broadcasted_iota(jnp.int32, (tok, tok), 1)
-        < lax.broadcasted_iota(jnp.int32, (tok, tok), 0),
-        1.0,
-        0.0,
-    )
-    before = jnp.dot(earlier.astype(bf16), member.astype(bf16), preferred_element_type=f32)
-    place = before + (lane ^ ep).astype(f32) * cap
-    place_first = jnp.sum(jnp.where(is_first, place, 0.0), axis=1, keepdims=True)
-    place_second = jnp.sum(jnp.where(is_second, place, 0.0), axis=1, keepdims=True)
-    slots = lax.broadcasted_iota(jnp.int32, (tok, n_ep * cap), 1).astype(f32)
-    at_first, at_second = slots == place_first, slots == place_second
-    select = (jnp.where(at_first, 1.0, 0.0) + jnp.where(at_second, 1.0, 0.0)).astype(bf16)
+    row_first, row_second = places(
+        (n_ep, tok), 1, routes[0:1], routes[1:2],
+        lambda member: jnp.dot(member, later, preferred_element_type=f32),
+    )
+    select = (
+        jnp.where(slots == row_first, 1.0, 0.0) + jnp.where(slots == row_second, 1.0, 0.0)
+    ).astype(bf16)
     inputs[1].wait()
-    chosen = lax.dot_general(
-        select, tokens_ref[...], (((0,), (0,)), ((), ())), preferred_element_type=f32
-    ).astype(bf16)
+    chosen = jnp.dot(select, tokens_ref[...], preferred_element_type=f32).astype(bf16)
     xall[pl.ds(tp, 1), 0] = chosen[:cap][None]
     picked[...] = chosen
     inputs[2].wait()
@@ -367,9 +372,9 @@
             returned[d].start()
 
     def mixing(d0, d1):
-        cols = slice(d0 * cap, d1 * cap)
-        part = jnp.where(at_first[:, cols], column(gates[0:1]), 0.0) + jnp.where(
-            at_second[:, cols], column(gates[1:2]), 0.0
+        slot = lax.broadcasted_iota(jnp.int32, (tok, (d1 - d0) * cap), 1).astype(f32) + d0 * cap
+        part = jnp.where(slot == column(row_first), column(gates[0:1]), 0.0) + jnp.where(
+            slot == column(row_second), column(gates[1:2]), 0.0
         )
         high = part.astype(bf16)
         low = (part - high.astype(f32)).astype(bf16)
@@ -378,9 +383,9 @@
     def gather(d0, d1):
         if d0 == 0:
             inputs[3].wait()
+        high, low = mixing(d0, d1)
         lo = max(d0, 1)
         wait_bytes(back.at[pl.ds(lo * cap, (d1 - lo) * cap)], ret_r.at[part_of[lo]])
-        high, low = mixing(d0, d1)
         rows = back[d0 * cap : d1 * cap]
         total = jnp.dot(high, rows, preferred_element_type=f32) + jnp.dot(
             low, rows, preferred_element_type=f32
@@ -434,7 +439,7 @@
     top_count = routes.shape[1]
     cap = 2 * top_count * tok // n_ep
     _, d_model, ff = w_gate.shape
-    groups = [(0,1),(2,4),(3,5),(6,7)]
+    groups = GROUPS
     bf16, f32 = jnp.bfloat16, jnp.float32
     dma = pltpu.SemaphoreType.DMA
     vmem = pl.BlockSpec(memory_space=pltpu.VMEM)
@@ -502,7 +507,7 @@
         P("tp"),
     )
     n_ep = mesh.shape["ep"]
-    pairs = mesh.shape["tp"] == 2 * CORES and n_ep >= 8 and n_ep & (n_ep - 1) == 0
+    pairs = mesh.shape["tp"] == 2 * CORES and n_ep == sum(map(len, GROUPS))
     return jax.shard_map(
         fused if pairs else shards, mesh=mesh, in_specs=placed, out_specs=P("ep", "tp"), check_vma=False
     )

time: 45.3 us -> 43.8 us (0.967)
  Pallas kernels: 44.5 us -> 43 us
    pallas_call x1, Pallas kernels: 44.5 us -> 43 us  [fused(): pl.pallas_call(functools.partial(layer, n_ep, cap, groups), out_shape=jax...]
where the time goes in v3:
time: 43.8 us; the launch traced here: 43.7 us
  Pallas kernels  43 us (98%)
  local copies, waits for them, and re-layouts  0.66 us (2%)
    pallas_call x1, Pallas kernels, fused(): pl.pallas_call(functools.partial(layer, n_ep, cap, groups), out_shape=jax...  43 us

profile of v3, /device:TPU:0, one launch (start us, length us, event | category | flops | bytes accessed | tf_op | source)
XLA Modules:
  0.0 43.7 jit_solution(6302092779979832358)
XLA Ops:
  0.0 43.0 %shard_map.82 = bf16[128,512]{1,0:T(8,128)(2,1)S(1)} custom-call(s32[2,128]{1,0:T(2,128)} %bitcast.2, f32[2,128]{1,0:T(2,128)} %bitcast.3, bf16[128,512]{1,0:T(8,128)(2,1)} %tokens_hbm.1, bf16[512]{0:T(512)(128)(2,1)} %in_gain_hbm.1, bf16[512]{0:T(512)(128)(2,1)} %out_gain_hbm.1, bf16[1,2048,1024]{2,1,0:T(8,128)(2,1)} %wg_hbm.1, ...), custom_call_target="tpu_custom_call" | custom-call | tf_op jit(solution)/shard_map/pallas_call | solution.py:448
  43.0 0.7 %copy.10 = bf16[128,512]{1,0:T(8,128)(2,1)} copy(bf16[128,512]{1,0:T(8,128)(2,1)S(1)} %shard_map.82) | data formatting | bytes 262144
